TPU v7x, 32 devices: a whole 2x2x4 slice. The times are simulated.
32 devices in a mesh: ep: 4 (over y, x), tp: 8 (over z, core).
Axes of the slice: x: 2, y: 2, z: 4, core: 2. Of those that a mesh axis runs over, the one named last changes fastest.
Arguments:
- tokens: bfloat16 [128, 4096], P('ep'), may hold values from -6 to 6
- norm_gain: float32 [4096], replicated, may hold values from 0.1 to 1.9
- group_ids: int32 [128, 1], P('ep'), may hold values from 0 to 1; in each aligned block of 32 rows (0 to 31, 32 to 63, ...) at most 32 rows name the same one
- local_ids: int32 [128, 4], P('ep'), may hold values from 0 to 7, all different within a row
- group_gate: float32 [128], P('ep'), may hold values from 0.3 to 1
- expert_gate: float32 [128, 4], P('ep'), may hold values from 0.1 to 1
- lengths: int32 [32], P('ep'), may hold values from 1 to 4, 64 in all
- w_gate: bfloat16 [16, 1024, 4096], P('ep', 'tp'), may hold values from -0.09375 to 0.09375
- w_up: bfloat16 [16, 1024, 4096], P('ep', 'tp'), may hold values from -0.09375 to 0.09375
- w_down: bfloat16 [16, 1024, 4096], P('ep', None, 'tp'), may hold values from -0.1875 to 0.1875
Outputs:
- mixed: bfloat16 [128, 4096], P('ep', 'tp')
Inputs may be any that keep to these rules, and one draw needn't show every extreme that they name: `group_ids`: among the 32 rows of one index of ep no group is named by more than 32 rows, and some index reaches 32. `local_ids`: each row names 4 different experts of its group. `lengths`: the first that many of a sequence's 4 positions are live.
All inputs are finite; a program needn't handle non-finite values. No bound on the sum of `lengths` on one device may be relied on, other than what follows from the above.
Results may differ from a plain program's by a relative error of at most 0.0065.
Values may be sent and summed in bfloat16 or wider, within the bound.
A program may use at most 64 MiB of HBM per device.

v0:
```python
import jax
import jax.numpy as jnp
from jax import lax
from jax.sharding import PartitionSpec as P

EXP_PER_GROUP = 8
STEP_TOK = 4


def norm_rows(tokens, norm_gain):
    values = tokens.astype(jnp.float32)
    scale = lax.rsqrt(jnp.mean(values * values, axis=1, keepdims=True) + 1e-06)
    return (values * scale * norm_gain).astype(jnp.bfloat16)


def live_mask(lengths, tok_rows):
    places = jnp.arange(tok_rows, dtype=jnp.int32)
    within = places % STEP_TOK
    owner = places // STEP_TOK
    seq_ids = jnp.arange(lengths.shape[0], dtype=jnp.int32)
    hits = (owner[:, None] == seq_ids[None, :]) & (within[:, None] < lengths[None, :])
    return jnp.any(hits, axis=1).astype(jnp.float32)


def expert_hidden(rows, w_gate, w_up):
    gate_part = jnp.einsum("rd,efd->ref", rows, w_gate, preferred_element_type=jnp.float32)
    up_part = jnp.einsum("rd,efd->ref", rows, w_up, preferred_element_type=jnp.float32)
    return (jax.nn.silu(gate_part) * up_part).astype(jnp.bfloat16)


def local(
    tokens, norm_gain, group_ids, local_ids, group_gate, expert_gate, lengths, w_gate, w_up, w_down
):
    highest = lax.Precision.HIGHEST
    tok_rows = tokens.shape[0]
    exp_dev = w_gate.shape[0]
    width_part = w_down.shape[2]
    ep_size = lax.axis_size("ep")
    groups = exp_dev * ep_size // EXP_PER_GROUP
    normed = norm_rows(tokens, norm_gain)
    live = live_mask(lengths, tok_rows)
    local_cols = jnp.arange(EXP_PER_GROUP, dtype=jnp.int32)
    picks = (local_ids[:, :, None] == local_cols[None, None, :]).astype(jnp.float32)
    weights = expert_gate * (group_gate * live)[:, None]
    dense = jnp.sum(picks * weights[:, :, None], axis=1)
    group_cols = jnp.arange(groups, dtype=jnp.int32)
    member_int = (group_ids == group_cols[None, :]).astype(jnp.int32)
    member = member_int.astype(jnp.float32)
    capacity = 2 * tok_rows // groups
    counts = jnp.cumsum(member_int, axis=0)
    rank = jnp.sum((counts - 1) * member_int, axis=1)
    slot_ids = jnp.arange(capacity, dtype=jnp.int32)
    select = member.T[:, None, :] * (rank[None, None, :] == slot_ids[None, :, None]).astype(
        jnp.float32
    )
    rows_by_group = jnp.einsum(
        "gct,td->gcd", select.astype(jnp.bfloat16), normed, preferred_element_type=jnp.float32
    ).astype(jnp.bfloat16)
    gates_by_group = jnp.einsum("gct,tl->gcl", select, dense, precision=highest)
    share = EXP_PER_GROUP // exp_dev
    send_rows = jnp.repeat(rows_by_group, share, axis=0)
    send_gates = gates_by_group.reshape(groups, capacity, share, exp_dev).transpose(0, 2, 1, 3)
    send_gates = send_gates.reshape(ep_size, capacity, exp_dev)
    recv_rows = lax.all_to_all(send_rows, "ep", split_axis=0, concat_axis=0, tiled=True)
    recv_gates = lax.all_to_all(send_gates, "ep", split_axis=0, concat_axis=0, tiled=True)
    slot_rows = recv_rows.reshape(ep_size * capacity, recv_rows.shape[2])
    slot_gates = recv_gates.reshape(ep_size * capacity, exp_dev)
    hidden = expert_hidden(slot_rows, w_gate, w_up)
    total = jnp.einsum(
        "ref,efd->red",
        lax.all_gather(hidden, "tp", axis=2, tiled=True),
        w_down,
        preferred_element_type=jnp.float32,
    )
    results = jnp.einsum("re,red->rd", slot_gates, total, precision=highest)
    results = results.reshape(ep_size, capacity, width_part)
    back = lax.all_to_all(results, "ep", split_axis=0, concat_axis=0, tiled=True)
    grouped = jnp.sum(back.reshape(groups, share, capacity, width_part), axis=1)
    mixed = jnp.einsum("gct,gcd->td", select, grouped, precision=highest)
    return mixed.astype(jnp.bfloat16)


def solution(mesh):
    in_specs = (
        P("ep", None),
        P(),
        P("ep", None),
        P("ep", None),
        P("ep"),
        P("ep", None),
        P("ep"),
        P("ep", "tp", None),
        P("ep", "tp", None),
        P("ep", None, "tp"),
    )
    out_specs = P("ep", "tp")
    return jax.shard_map(local, mesh=mesh, in_specs=in_specs, out_specs=out_specs, check_vma=False)
```

profile of v0, /device:TPU:0, one launch (start us, length us, event | category | flops | bytes accessed | tf_op | source)
XLA Modules:
  0.0 81.1 jit_solution(2347612556403566781)
XLA Ops:
  6.5 0.7 fusion.25
  7.2 0.7 fusion.17
  7.9 1.1 %fusion.4 = f32[32]{0:T(128)S(1)} fusion(bf16[32,4096]{1,0:T(8,128)(2,1)} %param.10), kind=kLoop, calls=%fused_computation.10 | loop fusion | flops 393184 | bytes 262272 | tf_op jit(solution)/shard_map/reduce_sum | solution.py:12
  9.0 0.1 reduce_window_sum.11
  9.1 1.0 %select_reduce_fusion.1 = s32[32]{0:T(128)S(1)} fusion(s32[32,2]{1,0:T(8,128)S(1)} %reduce_window_sum.11, s32[32]{0:T(128)} %bitcast.46), kind=kLoop, calls=%fused_computation.27 | loop fusion | flops 224 | bytes 512 | tf_op jit(solution)/shard_map/reduce_sum | solution.py:51
  10.1 0.1 fusion.21
  10.2 1.6 %convolution_convert_fusion = bf16[2,32,4096]{2,1,0:T(8,128)(2,1)S(1)} fusion(bf16[32,4096]{1,0:T(8,128)(2,1)} %param.10, f32[4096]{0:T(1024)} %param.11, f32[32]{0:T(128)S(1)} %add_rsqrt_fusion, f32[32,32]{0,1:T(8,128)S(1)} %fusion.21, f32[2,32]{1,0:T(2,128)S(1)} %fusion.25), kind=kOutput, calls=%fused_computation | convolution fusion | flops 17567744 | bytes 807296 | tf_op jit(solution)/shard_map/gct,td->gcd/dot_general | solution.py:56
  11.7 0.1 broadcast_in_dim.2
  11.8 0.0 copy-start.4
  11.8 19.4 %all_to_all.15 = bf16[4,32,4096]{2,1,0:T(8,128)(2,1)S(1)} all-to-all(bf16[4,32,4096]{2,1,0:T(8,128)(2,1)S(1)} %bitcast.37), channel_id=1, replica_groups=mesh['ep'=4,'tp'=8] {'ep'}, dimensions={0} | all-to-all | bytes 2097152 | tf_op jit(solution)/shard_map/all_to_all | solution.py:64
  31.3 1.5 %fusion.27 = f32[128,4,128]{2,0,1:T(8,128)S(1)} fusion(bf16[128,4096,1]{1,0,2:T(8,128)(2,1)S(1)} %bitcast.38, bf16[4,128,4096]{2,1,0:T(8,128)(2,1)S(1)} %copy-done), kind=kOutput, calls=%fused_computation.51 | convolution fusion | flops 536870912 | bytes 5505024 | tf_op jit(solution)/shard_map/rd,efd->ref/dot_general | solution.py:26
  32.8 0.0 copy-start.3
  32.8 0.0 copy-start.5
  32.8 0.0 copy-start.1
  32.8 0.0 copy-start.2
  32.8 2.2 %fusion = bf16[128,4,128]{2,0,1:T(8,128)(2,1)} fusion(bf16[128,4096,1]{1,0,2:T(8,128)(2,1)S(1)} %bitcast.39, bf16[4,128,4096]{2,1,0:T(8,128)(2,1)S(1)} %copy-done.4, f32[128,4,128]{2,0,1:T(8,128)S(1)} %fusion.27), kind=kOutput, calls=%fused_computation.3 | convolution fusion | flops 537264128 | bytes 5636096 | tf_op jit(solution)/shard_map/rd,efd->ref/dot_general | solution.py:27
  35.0 0.0 all-gather.2.cloned.1.call-update
  35.1 0.1 fusion.24
  35.2 0.2 fusion.12
  35.4 0.1 pad_maximum_fusion
  35.5 0.1 reshape.102
  35.6 0.1 reshape.115
  35.7 7.0 %all_to_all.16 = f32[4,1,128]{2,1,0:T(1,128)S(1)} all-to-all(f32[4,1,128]{2,1,0:T(1,128)S(1)} %reshape.115), channel_id=1, replica_groups=mesh['ep'=4,'tp'=8] {'ep'}, dimensions={0} | all-to-all | bytes 4096 | tf_op jit(solution)/shard_map/all_to_all | solution.py:65
  42.7 0.5 broadcast.120
  43.2 0.7 reduce
  43.9 0.1 reshape.116
  44.0 0.1 copy.43
  44.1 14.7 %all-gather.2.cloned.1.call-done = bf16[128,4,1024]{2,0,1:T(8,128)(2,1)} async-done(((bf16[128,4,128]{2,0,1:T(8,128)(2,1)}), bf16[128,4,1024]{2,0,1:T(8,128)(2,1)}) %all-gather.2.cloned.1.call-update) | async-done | bytes 1048592 | tf_op jit(solution)/shard_map/all_gather | solution.py:71
  58.8 3.2 %convolution_bitcast_fusion = f32[128,4,512]{2,0,1:T(8,128)S(1)} fusion(bf16[128,4,1024]{2,0,1:T(8,128)(2,1)} %all-gather.2.cloned.1.call-done, bf16[4,1024,512]{2,1,0:T(8,128)(2,1)} %param.19), kind=kOutput, calls=%fused_computation.1 | convolution fusion | flops 536870912 | bytes 6291456 | tf_op jit(solution)/shard_map/ref,efd->red/dot_general | solution.py:69
  62.0 2.4 %fusion.2 = f32[128,1,512]{2,1,0:T(1,128)S(1)} fusion(f32[128,4,1]{1,2,0:T(1,128)S(1)} %bitcast.41, f32[128,4,512]{2,0,1:T(8,128)S(1)} %convolution_bitcast_fusion), kind=kOutput, calls=%fused_computation.6 | convolution fusion | flops 3145728 | bytes 1312768 | tf_op jit(solution)/shard_map/re,red->rd/dot_general | solution.py:75
  64.5 8.8 %all_to_all.17 = f32[4,32,512]{2,1,0:T(8,128)S(1)} all-to-all(f32[4,32,512]{2,1,0:T(8,128)S(1)} %bitcast.40), channel_id=1, replica_groups=mesh['ep'=4,'tp'=8] {'ep'}, dimensions={0} | all-to-all | bytes 524288 | tf_op jit(solution)/shard_map/all_to_all | solution.py:77
  73.3 0.9 %fusion.1 = bf16[32,512]{1,0:T(8,128)(2,1)} fusion(f32[2,32,512]{2,1,0:T(8,128)S(1)} %bitcast_reduce_fusion, f32[32,32]{0,1:T(8,128)S(1)} %fusion.21, f32[2,32]{1,0:T(2,128)S(1)} %fusion.25), kind=kOutput, calls=%fused_computation.5 | convolution fusion | flops 12601344 | bytes 168192 | tf_op jit(solution)/shard_map/gct,gcd->td/dot_general | solution.py:79
  (18 shorter events, 0.1 us)
Async XLA Ops:
  6.5 52.3 %all-gather.2.cloned.1.call-start = ((), (), s32[]{:S(2)}) async-start(), calls=%async_computation.3 | async-start | bytes 1179648 | tf_op jit(solution)/shard_map/all_gather | solution.py:71
  9.1 22.2 %copy-start = (bf16[4,128,4096]{2,1,0:T(8,128)(2,1)S(1)}, bf16[4,128,4096]{2,1,0:T(8,128)(2,1)}, u32[]{:S(2)}) copy-start(bf16[4,128,4096]{2,1,0:T(8,128)(2,1)} %param.17) | copy-start | bytes 12582916
  11.8 21.0 %copy-start.4 = (bf16[4,128,4096]{2,1,0:T(8,128)(2,1)S(1)}, bf16[4,128,4096]{2,1,0:T(8,128)(2,1)}, u32[]{:S(2)}) copy-start(bf16[4,128,4096]{2,1,0:T(8,128)(2,1)} %param.18) | copy-start | bytes 12582916
  32.8 2.3 %copy-start.3 = (s32[8]{0:T(128)S(1)}, s32[8]{0:T(128)}, u32[]{:S(2)}) copy-start(s32[8]{0:T(128)} %param.16) | copy-start | bytes 100
  32.8 2.4 %copy-start.5 = (f32[32]{0:T(128)S(1)}, f32[32]{0:T(128)}, u32[]{:S(2)}) copy-start(f32[32]{0:T(128)} %param.14) | copy-start | bytes 388
  32.8 2.4 %copy-start.1 = (f32[32,4]{0,1:T(4,128)S(1)}, f32[32,4]{0,1:T(4,128)}, u32[]{:S(2)}) copy-start(f32[32,4]{0,1:T(4,128)} %param.15) | copy-start | bytes 1540
  32.8 2.4 %copy-start.2 = (s32[32,4]{0,1:T(4,128)S(1)}, s32[32,4]{0,1:T(4,128)}, u32[]{:S(2)}) copy-start(s32[32,4]{0,1:T(4,128)} %param.13) | copy-start | bytes 1540
Sparse Core Ops, SparseCore 0:
  35.2 23.5 all-gather.1
where the time goes:
time: 81.4 us; the launch traced here: 81.1 us
  blocking collectives  35.2 us (43%)
  waiting for transfers between devices  14.7 us (18%)
  between operations  13.6 us (17%)
  matrix products  12.1 us (15%)
  other arithmetic  4.48 us (6%)
  local copies, waits for them, and re-layouts  1.06 us (1%)
    all_to_all x1, blocking collectives, local(): lax.all_to_all(send_rows, 'ep', split_axis=0, concat_axis=0, tiled=True)  19.4 us
    all_gather x1, waiting for transfers between devices, local(): lax.all_gather(hidden, 'tp', axis=2, tiled=True)  14.7 us
    all_to_all x1, blocking collectives, local(): lax.all_to_all(results, 'ep', split_axis=0, concat_axis=0, tiled=True)  8.79 us
    all_to_all x1, blocking collectives, local(): lax.all_to_all(send_gates, 'ep', split_axis=0, concat_axis=0, tiled=True)  7.01 us
    dot_general x1, matrix products, local(): jnp.einsum('ref,efd->red', lax.all_gather(hidden, 'tp', axis=2, tiled=Tru...  3.23 us
    dot_general x1, matrix products, local(): results = jnp.einsum('re,red->rd', slot_gates, total, precision=highest)  2.43 us
    dot_general x1, matrix products, expert_hidden(): jnp.einsum('rd,efd->ref', rows, w_up, preferred_element_type=jnp.float32)  2.18 us
  transfers between devices with their start and end apart: 1, of which 1 were waited for; matrix products, arithmetic and copies ran while one was open for 2% of the time, Pallas kernels for 0%

commit v1 on v0

--- a/solution.py
+++ b/solution.py
@@ -5,6 +5,25 @@
 
 EXP_PER_GROUP = 8
 STEP_TOK = 4
+
+
+def make_skins(piece_in, w_in):
+    parts_out = lax.axis_size("tp")
+    item_now, block_out, arr_next = (parts_out, lax.axis_index("tp"), piece_in.shape[2])
+    found = [(q, (q + 1) % item_now) for q in range(item_now)]
+    all_blocks = [(q, (q - 1) % item_now) for q in range(item_now)]
+    outcome_arr = item_now // 2
+    side_arr = view_out = piece_in
+    local_out = w_in(piece_in, block_out * arr_next)
+    rr = 1
+    while rr < outcome_arr + 1:
+        side_arr = lax.ppermute(side_arr, axis_name="tp", perm=found)
+        if rr < item_now - outcome_arr:
+            view_out = lax.ppermute(view_out, axis_name="tp", perm=all_blocks)
+            local_out = local_out + w_in(view_out, (block_out + rr) % item_now * arr_next)
+        local_out = local_out + w_in(side_arr, (block_out - rr) % item_now * arr_next)
+        rr += 1
+    return local_out
 
 
 def norm_rows(tokens, norm_gain):
@@ -66,11 +85,14 @@
     slot_rows = recv_rows.reshape(ep_size * capacity, recv_rows.shape[2])
     slot_gates = recv_gates.reshape(ep_size * capacity, exp_dev)
     hidden = expert_hidden(slot_rows, w_gate, w_up)
-    total = jnp.einsum(
-        "ref,efd->red",
-        lax.all_gather(hidden, "tp", axis=2, tiled=True),
-        w_down,
-        preferred_element_type=jnp.float32,
+    total = make_skins(
+        hidden,
+        lambda part, offset: jnp.einsum(
+            "ref,efd->red",
+            part,
+            lax.dynamic_slice_in_dim(w_down, offset, part.shape[2], axis=1),
+            preferred_element_type=jnp.float32,
+        ),
     )
     results = jnp.einsum("re,red->rd", slot_gates, total, precision=highest)
     results = results.reshape(ep_size, capacity, width_part)

time: 81.4 us -> 76.6 us (0.941)
  blocking collectives: 35.2 us -> 8.11 us
  starting transfers between devices: 0.01 us -> 18.2 us
  waiting for transfers between devices: 14.7 us -> 29.2 us
  between operations: 13.6 us -> 0.29 us
  other arithmetic: 4.48 us -> 7 us
  local copies, waits for them, and re-layouts: 1.06 us -> 2.71 us
  matrix products: 12.1 us -> 10.7 us
    all_to_all x2 -> x0, blocking collectives: 26.4 us -> none  [the longest x1 19.4 us: local(): lax.all_to_all(send_rows, 'ep', split_axis=0, concat_axis=0, tiled=True)]
    ppermute x0 -> x7, waiting for transfers between devices: none -> 16.1 us  [the longest x4 16.1 us: make_skins(): side_arr = lax.ppermute(side_arr, axis_name='tp', perm=found)]
    all_gather x1 -> x0, waiting for transfers between devices: 14.7 us -> none  [local(): lax.all_gather(hidden, 'tp', axis=2, tiled=True)]
    all_to_all x0 -> x2, waiting for transfers between devices: none -> 13.1 us  [the longest x1 11 us: local(): lax.all_to_all(send_rows, 'ep', split_axis=0, concat_axis=0, tiled=True)]
    ppermute x0 -> x7, starting transfers between devices: none -> 9.48 us  [the longest x3 9.47 us: make_skins(): view_out = lax.ppermute(view_out, axis_name='tp', perm=all_blocks)]
    all_to_all x0 -> x2, starting transfers between devices: none -> 8.71 us  [the longest x1 5.19 us: local(): lax.all_to_all(send_gates, 'ep', split_axis=0, concat_axis=0, tiled=True)]
    dot_general x2 -> x8, matrix products: 5.65 us -> 2.83 us  [local(): jnp.einsum('ref,efd->red', part, lax.dynamic_slice_in_dim(w_down, offset,...]
    dot_general x1, matrix products: 1.53 us -> 3.86 us  [expert_hidden(): jnp.einsum('rd,efd->ref', rows, w_gate, preferred_element_type=jnp.float32)]
  transfers between devices with their start and end apart: 1 -> 9, of which waited for: 1 -> 6; matrix products, arithmetic and copies ran while one was open for 2% -> 8% of each run, Pallas kernels for 0% -> 0%
where the time goes in v1:
time: 76.6 us; the launch traced here: 76.2 us
  waiting for transfers between devices  29.2 us (38%)
  starting transfers between devices  18.2 us (24%)
  matrix products  10.7 us (14%)
  blocking collectives  8.11 us (11%)
  other arithmetic  7 us (9%)
  local copies, waits for them, and re-layouts  2.71 us (4%)
    ppermute x4, waiting for transfers between devices, make_skins(): side_arr = lax.ppermute(side_arr, axis_name='tp', perm=found)  16.1 us
    all_to_all x1, waiting for transfers between devices, local(): lax.all_to_all(send_rows, 'ep', split_axis=0, concat_axis=0, tiled=True)  11 us
    ppermute x3, starting transfers between devices, make_skins(): view_out = lax.ppermute(view_out, axis_name='tp', perm=all_blocks)  9.47 us
    all_to_all x1, blocking collectives, local(): lax.all_to_all(results, 'ep', split_axis=0, concat_axis=0, tiled=True)  8.11 us
    all_to_all x1, starting transfers between devices, local(): lax.all_to_all(send_gates, 'ep', split_axis=0, concat_axis=0, tiled=True)  5.19 us
    dot_general x1, matrix products, expert_hidden(): jnp.einsum('rd,efd->ref', rows, w_gate, preferred_element_type=jnp.float32)  3.86 us
    all_to_all x1, starting transfers between devices, local(): lax.all_to_all(send_rows, 'ep', split_axis=0, concat_axis=0, tiled=True)  3.51 us
    dot_general x8, matrix products, local(): jnp.einsum('ref,efd->red', part, lax.dynamic_slice_in_dim(w_down, offset,...  2.83 us
  transfers between devices with their start and end apart: 9, of which 6 were waited for; matrix products, arithmetic and copies ran while one was open for 8% of the time, Pallas kernels for 0%

profile of v1, /device:TPU:0, one launch (start us, length us, event | category | flops | bytes accessed | tf_op | source)
XLA Modules:
  0.0 76.2 jit_solution(9749560860275209126)
XLA Ops:
  0.0 0.7 fusion.31
  0.7 0.7 fusion.47
  1.4 0.8 %select_reduce_fusion.1 = s32[32]{0:T(128)S(1)} fusion(s32[32,2]{1,0:T(8,128)S(1)} %reduce_window_sum.11, s32[32]{0:T(128)} %bitcast.52), kind=kLoop, calls=%fused_computation.45 | loop fusion | flops 224 | bytes 512 | tf_op jit(solution)/shard_map/reduce_sum | solution.py:70
  2.4 0.7 fusion.38
  3.1 0.7 broadcast_select_fusion
  3.8 0.7 broadcast_multiply_fusion
  4.4 0.7 select_reduce_fusion
  5.5 0.7 reshape.114
  6.2 5.2 %all-to-all-start = ((f32[4,1,128]{2,1,0:T(1,128)}), f32[4,1,128]{2,1,0:T(1,128)S(1)}, u32[]{:S(2)}, u32[]{:S(2)}) async-start(f32[4,1,128]{2,1,0:T(1,128)} %reshape.114), calls=%async_computation | async-start | bytes 4096 | tf_op jit(solution)/shard_map/all_to_all | solution.py:84
  11.4 1.1 %fusion.7 = f32[32]{0:T(128)S(1)} fusion(bf16[32,4096]{1,0:T(8,128)(2,1)} %param.10), kind=kLoop, calls=%fused_computation.17 | loop fusion | flops 393184 | bytes 262272 | tf_op jit(solution)/shard_map/reduce_sum | solution.py:31
  12.5 1.4 %convolution_convert_fusion = bf16[2,32,4096]{2,1,0:T(8,128)(2,1)S(1)} fusion(bf16[32,4096]{1,0:T(8,128)(2,1)} %param.10, f32[4096]{0:T(1024)} %param.11, f32[32]{0:T(128)S(1)} %add_rsqrt_fusion, f32[32,32]{0,1:T(8,128)S(1)} %fusion.35, f32[2,32]{1,0:T(2,128)S(1)} %fusion.47), kind=kOutput, calls=%fused_computation | convolution fusion | flops 17567744 | bytes 807296 | tf_op jit(solution)/shard_map/gct,td->gcd/dot_general | solution.py:75
  13.9 2.1 %all-to-all-done = f32[4,1,128]{2,1,0:T(1,128)S(1)} async-done(((f32[4,1,128]{2,1,0:T(1,128)}), f32[4,1,128]{2,1,0:T(1,128)S(1)}, u32[]{:S(2)}, u32[]{:S(2)}) %all-to-all-start) | async-done | bytes 2080 | tf_op jit(solution)/shard_map/all_to_all | solution.py:84
  16.0 1.1 %broadcast_in_dim.2 = bf16[2,2,32,4096]{3,2,1,0:T(8,128)(2,1)} broadcast(bf16[2,32,4096]{2,1,0:T(8,128)(2,1)S(1)} %convolution_convert_fusion), dimensions={0,2,3} | broadcast | bytes 1572864 | tf_op jit(solution)/shard_map/broadcast_in_dim | solution.py:80
  17.1 3.5 %all-to-all-start.1 = ((bf16[4,32,4096]{2,1,0:T(8,128)(2,1)}), bf16[4,32,4096]{2,1,0:T(8,128)(2,1)S(1)}, u32[]{:S(2)}, u32[]{:S(2)}) async-start(bf16[4,32,4096]{2,1,0:T(8,128)(2,1)} %bitcast.3), calls=%async_computation.1 | async-start | bytes 2097152 | tf_op jit(solution)/shard_map/all_to_all | solution.py:83
  20.7 0.5 broadcast.128
  21.3 0.7 reduce.2
  22.1 11.0 %all-to-all-done.1 = bf16[4,32,4096]{2,1,0:T(8,128)(2,1)S(1)} async-done(((bf16[4,32,4096]{2,1,0:T(8,128)(2,1)}), bf16[4,32,4096]{2,1,0:T(8,128)(2,1)S(1)}, u32[]{:S(2)}, u32[]{:S(2)}) %all-to-all-start.1) | async-done | bytes 1048608 | tf_op jit(solution)/shard_map/all_to_all | solution.py:83
  33.1 3.9 %fusion.49 = f32[128,4,128]{2,0,1:T(8,128)S(1)} fusion(bf16[128,4096,1]{1,0,2:T(8,128)(2,1)S(1)} %bitcast.45, bf16[4,128,4096]{2,1,0:T(8,128)(2,1)} %param.17), kind=kOutput, calls=%fused_computation.77 | convolution fusion | flops 536870912 | bytes 5505024 | tf_op jit(solution)/shard_map/rd,efd->ref/dot_general | solution.py:45
  37.0 1.5 %fusion.5 = bf16[128,4,128]{2,0,1:T(8,128)(2,1)S(1)} fusion(bf16[128,4096,1]{1,0,2:T(8,128)(2,1)S(1)} %bitcast.46, bf16[4,128,4096]{2,1,0:T(8,128)(2,1)S(1)} %copy-done.1, f32[128,4,128]{2,0,1:T(8,128)S(1)} %fusion.49), kind=kOutput, calls=%fused_computation.12 | convolution fusion | flops 537264128 | bytes 5636096 | tf_op jit(solution)/shard_map/rd,efd->ref/dot_general | solution.py:46
  38.5 2.3 %collective-permute-start = (bf16[128,4,128]{2,0,1:T(8,128)(2,1)S(1)}, bf16[128,4,128]{2,0,1:T(8,128)(2,1)S(1)}, u32[]{:S(2)}, u32[]{:S(2)}) collective-permute-start(bf16[128,4,128]{2,0,1:T(8,128)(2,1)S(1)} %fusion.5), channel_id=1, source_target_pairs={{0,7},{1,0},{2,1},{3,2},{4,3},{5,4},{6,5},{7,6},{8,15},{9,8},{10,9... | collective-permute-start | bytes 393224 | tf_op jit(solution)/shard_map/ppermute | solution.py:22
  41.2 5.8 %collective-permute-done.1 = bf16[128,4,128]{2,0,1:T(8,128)(2,1)S(1)} collective-permute-done((bf16[128,4,128]{2,0,1:T(8,128)(2,1)S(1)}, bf16[128,4,128]{2,0,1:T(8,128)(2,1)S(1)}, u32[]{:S(2)}, u32[]{:S(2)}) %collective-permute-start.1) | collective-permute-done | bytes 131104 | tf_op jit(solution)/shard_map/ppermute | solution.py:20
  47.0 3.5 %collective-permute-start.2 = (bf16[128,4,128]{2,0,1:T(8,128)(2,1)S(1)}, bf16[128,4,128]{2,0,1:T(8,128)(2,1)S(1)}, u32[]{:S(2)}, u32[]{:S(2)}) collective-permute-start(bf16[128,4,128]{2,0,1:T(8,128)(2,1)S(1)} %collective-permute-done), channel_id=1, source_target_pairs={{0,7},{1,0},{2,1},{3,2},{4,3},{5,4},{6,5},{7,6},{8,15},{9,8},{10,9... | collective-permute-start | bytes 393224 | tf_op jit(solution)/shard_map/ppermute | solution.py:22
  50.9 0.4 convolution_add_fusion.3
  51.3 2.9 %collective-permute-done.3 = bf16[128,4,128]{2,0,1:T(8,128)(2,1)S(1)} collective-permute-done((bf16[128,4,128]{2,0,1:T(8,128)(2,1)S(1)}, bf16[128,4,128]{2,0,1:T(8,128)(2,1)S(1)}, u32[]{:S(2)}, u32[]{:S(2)}) %collective-permute-start.3) | collective-permute-done | bytes 131104 | tf_op jit(solution)/shard_map/ppermute | solution.py:20
  54.6 3.6 %collective-permute-start.4 = (bf16[128,4,128]{2,0,1:T(8,128)(2,1)S(1)}, bf16[128,4,128]{2,0,1:T(8,128)(2,1)S(1)}, u32[]{:S(2)}, u32[]{:S(2)}) collective-permute-start(bf16[128,4,128]{2,0,1:T(8,128)(2,1)S(1)} %collective-permute-done.2), channel_id=1, source_target_pairs={{0,7},{1,0},{2,1},{3,2},{4,3},{5,4},{6,5},{7,6},{8,15},{9,8},{10,9... | collective-permute-start | bytes 393224 | tf_op jit(solution)/shard_map/ppermute | solution.py:22
  58.2 0.4 fusion.3
  58.5 1.9 %collective-permute-done.5 = bf16[128,4,128]{2,0,1:T(8,128)(2,1)S(1)} collective-permute-done((bf16[128,4,128]{2,0,1:T(8,128)(2,1)S(1)}, bf16[128,4,128]{2,0,1:T(8,128)(2,1)S(1)}, u32[]{:S(2)}, u32[]{:S(2)}) %collective-permute-start.5) | collective-permute-done | bytes 131104 | tf_op jit(solution)/shard_map/ppermute | solution.py:20
  60.8 0.4 fusion.2
  61.1 5.5 %collective-permute-done.6 = bf16[128,4,128]{2,0,1:T(8,128)(2,1)S(1)} collective-permute-done((bf16[128,4,128]{2,0,1:T(8,128)(2,1)S(1)}, bf16[128,4,128]{2,0,1:T(8,128)(2,1)S(1)}, u32[]{:S(2)}, u32[]{:S(2)}) %collective-permute-start.6) | collective-permute-done | bytes 131104 | tf_op jit(solution)/shard_map/ppermute | solution.py:20
  66.6 0.4 fusion.4
  67.1 8.1 %all_to_all.15 = f32[4,32,512]{2,1,0:T(8,128)S(1)} all-to-all(f32[4,32,512]{2,1,0:T(8,128)S(1)} %bitcast.47), channel_id=1, replica_groups=mesh['ep'=4,'tp'=8] {'ep'}, dimensions={0} | all-to-all | bytes 524288 | tf_op jit(solution)/shard_map/all_to_all | solution.py:99
  75.2 0.9 %fusion.6 = bf16[32,512]{1,0:T(8,128)(2,1)} fusion(f32[2,32,512]{2,1,0:T(8,128)S(1)} %bitcast_reduce_fusion, f32[32,32]{0,1:T(8,128)S(1)} %fusion.35, f32[2,32]{1,0:T(2,128)S(1)} %fusion.47), kind=kOutput, calls=%fused_computation.14 | convolution fusion | flops 12601344 | bytes 168192 | tf_op jit(solution)/shard_map/gct,gcd->td/dot_general | solution.py:101
  (30 shorter events, 2.3 us)
Async XLA Ops:
  6.2 9.8 %all-to-all-start = ((f32[4,1,128]{2,1,0:T(1,128)}), f32[4,1,128]{2,1,0:T(1,128)S(1)}, u32[]{:S(2)}, u32[]{:S(2)}) async-start(f32[4,1,128]{2,1,0:T(1,128)} %reshape.114), calls=%async_computation | async-start | bytes 4096 | tf_op jit(solution)/shard_map/all_to_all | solution.py:84
  17.1 16.0 %all-to-all-start.1 = ((bf16[4,32,4096]{2,1,0:T(8,128)(2,1)}), bf16[4,32,4096]{2,1,0:T(8,128)(2,1)S(1)}, u32[]{:S(2)}, u32[]{:S(2)}) async-start(bf16[4,32,4096]{2,1,0:T(8,128)(2,1)} %bitcast.3), calls=%async_computation.1 | async-start | bytes 2097152 | tf_op jit(solution)/shard_map/all_to_all | solution.py:83
  33.1 3.9 %copy-start.1 = (bf16[4,128,4096]{2,1,0:T(8,128)(2,1)S(1)}, bf16[4,128,4096]{2,1,0:T(8,128)(2,1)}, u32[]{:S(2)}) copy-start(bf16[4,128,4096]{2,1,0:T(8,128)(2,1)} %param.18) | copy-start | bytes 12582916
  36.9 3.9 %copy-start = (bf16[4,1024,512]{2,1,0:T(8,128)(2,1)S(1)}, bf16[4,1024,512]{2,1,0:T(8,128)(2,1)}, u32[]{:S(2)}) copy-start(bf16[4,1024,512]{2,1,0:T(8,128)(2,1)} %param.19) | copy-start | bytes 12582916
  38.5 8.5 %collective-permute-start = (bf16[128,4,128]{2,0,1:T(8,128)(2,1)S(1)}, bf16[128,4,128]{2,0,1:T(8,128)(2,1)S(1)}, u32[]{:S(2)}, u32[]{:S(2)}) collective-permute-start(bf16[128,4,128]{2,0,1:T(8,128)(2,1)S(1)} %fusion.5), channel_id=1, source_target_pairs={{0,7},{1,0},{2,1},{3,2},{4,3},{5,4},{6,5},{7,6},{8,15},{9,8},{10,9... | collective-permute-start | bytes 393224 | tf_op jit(solution)/shard_map/ppermute | solution.py:22
  40.8 6.2 %collective-permute-start.1 = (bf16[128,4,128]{2,0,1:T(8,128)(2,1)S(1)}, bf16[128,4,128]{2,0,1:T(8,128)(2,1)S(1)}, u32[]{:S(2)}, u32[]{:S(2)}) collective-permute-start(bf16[128,4,128]{2,0,1:T(8,128)(2,1)S(1)} %fusion.5), channel_id=1, source_target_pairs={{0,1},{1,2},{2,3},{3,4},{4,5},{5,6},{6,7},{7,0},{8,9},{9,10},{10,1... | collective-permute-start | bytes 393224 | tf_op jit(solution)/shard_map/ppermute | solution.py:20
  47.0 7.2 %collective-permute-start.3 = (bf16[128,4,128]{2,0,1:T(8,128)(2,1)S(1)}, bf16[128,4,128]{2,0,1:T(8,128)(2,1)S(1)}, u32[]{:S(2)}, u32[]{:S(2)}) collective-permute-start(bf16[128,4,128]{2,0,1:T(8,128)(2,1)S(1)} %collective-permute-done.1), channel_id=1, source_target_pairs={{0,1},{1,2},{2,3},{3,4},{4,5},{5,6},{6,7},{7,0},{8,9},{9,10},{10,1... | collective-permute-start | bytes 393224 | tf_op jit(solution)/shard_map/ppermute | solution.py:20
  47.0 7.6 %collective-permute-start.2 = (bf16[128,4,128]{2,0,1:T(8,128)(2,1)S(1)}, bf16[128,4,128]{2,0,1:T(8,128)(2,1)S(1)}, u32[]{:S(2)}, u32[]{:S(2)}) collective-permute-start(bf16[128,4,128]{2,0,1:T(8,128)(2,1)S(1)} %collective-permute-done), channel_id=1, source_target_pairs={{0,7},{1,0},{2,1},{3,2},{4,3},{5,4},{6,5},{7,6},{8,15},{9,8},{10,9... | collective-permute-start | bytes 393224 | tf_op jit(solution)/shard_map/ppermute | solution.py:22
  54.2 6.2 %collective-permute-start.5 = (bf16[128,4,128]{2,0,1:T(8,128)(2,1)S(1)}, bf16[128,4,128]{2,0,1:T(8,128)(2,1)S(1)}, u32[]{:S(2)}, u32[]{:S(2)}) collective-permute-start(bf16[128,4,128]{2,0,1:T(8,128)(2,1)S(1)} %collective-permute-done.3), channel_id=1, source_target_pairs={{0,1},{1,2},{2,3},{3,4},{4,5},{5,6},{6,7},{7,0},{8,9},{9,10},{10,1... | collective-permute-start | bytes 393224 | tf_op jit(solution)/shard_map/ppermute | solution.py:20
  54.6 6.2 %collective-permute-start.4 = (bf16[128,4,128]{2,0,1:T(8,128)(2,1)S(1)}, bf16[128,4,128]{2,0,1:T(8,128)(2,1)S(1)}, u32[]{:S(2)}, u32[]{:S(2)}) collective-permute-start(bf16[128,4,128]{2,0,1:T(8,128)(2,1)S(1)} %collective-permute-done.2), channel_id=1, source_target_pairs={{0,7},{1,0},{2,1},{3,2},{4,3},{5,4},{6,5},{7,6},{8,15},{9,8},{10,9... | collective-permute-start | bytes 393224 | tf_op jit(solution)/shard_map/ppermute | solution.py:22
  60.4 6.2 %collective-permute-start.6 = (bf16[128,4,128]{2,0,1:T(8,128)(2,1)S(1)}, bf16[128,4,128]{2,0,1:T(8,128)(2,1)S(1)}, u32[]{:S(2)}, u32[]{:S(2)}) collective-permute-start(bf16[128,4,128]{2,0,1:T(8,128)(2,1)S(1)} %collective-permute-done.5), channel_id=1, source_target_pairs={{0,1},{1,2},{2,3},{3,4},{4,5},{5,6},{6,7},{7,0},{8,9},{9,10},{10,1... | collective-permute-start | bytes 393224 | tf_op jit(solution)/shard_map/ppermute | solution.py:20
